TPU v7x, 32 devices: a whole 2x2x4 slice. The times are simulated.
32 devices in a mesh: fs: 8 (over z, x), tp: 4 (over y, core).
Axes of the slice: x: 2, y: 2, z: 4, core: 2. Of those that a mesh axis runs over, the one named last changes fastest.
Arguments:
- tokens: bfloat16 [8192, 2048], P(('fs', 'tp')), may hold values from -130 to 130
- pool_weight: bfloat16 [4, 512, 512], P(None, 'fs'), may hold values from -0.25 to 0.25
- pool_scale: float32 [2048], replicated, may hold values from 0.5 to 1.5
- gain_mix: float32 [2048], replicated, may hold values from 0.1 to 1.9
- gain_mlp: float32 [2048], replicated, may hold values from 0.1 to 1.9
- w_up: bfloat16 [8192, 2048], P('tp', 'fs'), may hold values from -0.125 to 0.125
- w_down: bfloat16 [8192, 2048], P('tp', 'fs'), may hold values from -0.0625 to 0.0625
- gain_out: float32 [2048], P('tp'), may hold values from 0.1 to 1.9
Outputs:
- result: bfloat16 [8192, 2048], P('fs', 'tp')
All inputs are finite; a program needn't handle non-finite values.
Results may differ from a plain program's by a relative error of at most 0.013.
Values may be sent and summed in bfloat16 or wider, within the bound.
A program may use at most 64 MiB of HBM per device.

v0:
```python
import functools

import jax
import jax.numpy as jnp
from jax import lax
from jax.experimental import pallas as pl
from jax.experimental.pallas import tpu as pltpu
from jax.sharding import PartitionSpec as P

SEQ_LEN = 1024
EPS = 1e-06
WINDOWS = (2, 4, 8, 16)
HALO = 16
MESH = pl.DeviceIdType.MESH
POOL, UP, DOWN = 0, 1, 2


def ring_order(n, nx):
    nz = n // nx
    if nx < 2 or nz < 2 or nz % 2:
        return list(range(n))
    order = []
    for z in range(nz):
        xs = list(range(1, nx))
        order += [z * nx + x for x in (xs if z % 2 == 0 else xs[::-1])]
    return order + [z * nx for z in range(nz - 1, -1, -1)]


def lookup(table, index):
    value = jnp.int32(table[0])
    for i in range(1, len(table)):
        value = jnp.where(index == i, jnp.int32(table[i]), value)
    return value


def kernel(
    n, tp, order, tok_ref, pool_ref, up_ref, down_ref, scale_ref, gmix_ref, gmlp_ref,
    gout_ref, out_ref,
    pool_full, up_full, down_full, ext, first, inner_all, hidden, fcols, blocks, parts,
    before, after, edge, total, stat, stat_out, stat_in,
    ring_send, ring_recv, in_send, in_recv, fc_send, fc_recv, halo_send, halo_recv, rs_send, rs_recv,
    pair_send, pair_recv, st_send, st_recv,
):
    rows, width = tok_ref.shape
    group = width // 4
    hid, cols = up_ref.shape
    depth = pool_ref.shape[1]
    own_cols = width // tp
    per = n // tp
    seq = rows * tp
    me_fs, me = lax.axis_index("fs"), lax.axis_index("tp")
    place_of = [order.index(i) for i in range(n)]
    place = lookup(place_of, me_fs)

    def at(offset):
        return lookup(order, lax.rem(place + offset + 2 * n, n))

    owners = {0: me_fs}
    for d in range(1, n // 2 + 1):
        owners[d] = at(d)
        owners[-d] = at(-d)
    right, left = owners[1], owners[-1]

    barrier = pltpu.get_barrier_semaphore()
    for peer in (right, left):
        pl.semaphore_signal(barrier, inc=1, device_id={"fs": peer, "tp": me}, device_id_type=MESH)
    for d in range(1, tp):
        pl.semaphore_signal(
            barrier, inc=1, device_id={"fs": me_fs, "tp": lax.rem(me + d, tp)}, device_id_type=MESH
        )
    pl.semaphore_wait(barrier, 2 + tp - 1)

    hops = n // 2
    cores = 2 if tp % 2 == 0 else 1
    core = lax.rem(me, cores)
    lanes = 2 if cols % 256 == 0 else 1
    fine = cols // lanes

    def view(stream, full, owner, piece, sub=None):
        if stream == POOL:
            ref = pool_full if full else pool_ref
            half = ref.shape[0] // (2 * cores)
            r = pl.ds(pl.multiple_of(owner * depth, depth), depth) if full else slice(None)
            return ref.at[pl.ds((core * 2 + piece) * half, half), r, :]
        ref = (up_full if full else up_ref) if stream == UP else (down_full if full else down_ref)
        half = hid // 2
        c = pl.ds(pl.multiple_of(owner * cols, cols), cols) if full else slice(None)
        if sub is not None:
            c = pl.ds(pl.multiple_of(owner * cols + sub * fine, fine), fine)
        return ref.at[pl.ds(piece * half, half), c]

    def count(side, piece):
        return hops if piece == side else hops - 1

    def slot(stream, side, piece, hop, sub):
        if sub:
            return 12 * hops + side * (lanes - 1) + sub - 1
        return ((stream * 2 + side) * 2 + piece) * hops + hop

    def subs(stream, hop):
        return range(lanes) if stream == DOWN and hop == hops - 1 and hop > 0 else (None,)

    def ring(stream, side, piece, hop, sub):
        owner = owners[-hop] if side == 0 else owners[hop]
        return pltpu.make_async_remote_copy(
            src_ref=view(stream, hop > 0, owner, piece, sub),
            dst_ref=view(stream, True, owner, piece, sub),
            send_sem=ring_send.at[slot(stream, side, piece, hop, sub)],
            recv_sem=ring_recv.at[slot(stream, side, piece, hop, sub)],
            device_id={"fs": right if side == 0 else left, "tp": me},
            device_id_type=MESH,
        )

    started = []

    def arrived(stream, side, piece, hop, sub=None):
        owner = owners[-hop - 1] if side == 0 else owners[hop + 1]
        pltpu.make_async_remote_copy(
            src_ref=view(stream, True, owner, piece, sub),
            dst_ref=view(stream, True, owner, piece, sub),
            send_sem=ring_send.at[slot(stream, side, piece, hop, sub)],
            recv_sem=ring_recv.at[slot(stream, side, piece, hop, sub)],
            device_id={"fs": right if side == 0 else left, "tp": me},
            device_id_type=MESH,
        ).wait_recv()

    def start(stream, hop, which=(0, 1)):
        for w in which:
            for side in (0, 1):
                piece = side if w == 0 else 1 - side
                if hop < count(side, piece):
                    if hop > 0:
                        arrived(stream, side, piece, hop - 1)
                    for sub in subs(stream, hop):
                        copy = ring(stream, side, piece, hop, sub)
                        copy.start()
                        started.append(copy)

    def finish(stream, sub=None):
        for side in (0, 1):
            arrived(stream, side, side, hops - 1, sub)

    def settle(stream, hop):
        if hop == hops - 2:
            for side in (0, 1):
                arrived(stream, side, 1 - side, hop)

    start(POOL, 0)
    start(UP, 0, (0,))

    step = 32 if rows % 32 == 0 else rows

    @pl.loop(0, rows // step)
    def _(i):
        r = pl.ds(pl.multiple_of(i * step, step), step)
        x = tok_ref[r, :].astype(jnp.float32)
        y = x * lax.rsqrt(jnp.mean(x * x, axis=-1, keepdims=True) + EPS) * gmix_ref[...]
        y = y.astype(jnp.bfloat16)
        ext[pl.ds(pl.multiple_of(HALO + i * step, HALO), step), :] = y.astype(jnp.float32)

    edge[0] = ext[rows : rows + HALO, :].astype(jnp.bfloat16)
    edge[1] = ext[HALO : 2 * HALO, :].astype(jnp.bfloat16)
    halos = []
    for side, (buffer, d) in enumerate(((before, 1), (after, tp - 1))):
        copy = pltpu.make_async_remote_copy(
            src_ref=edge.at[side],
            dst_ref=buffer,
            send_sem=halo_send.at[side],
            recv_sem=halo_recv.at[side],
            device_id={"fs": me_fs, "tp": lax.rem(me + d, tp)},
            device_id_type=MESH,
        )
        copy.start()
        halos.append(copy)

    start(POOL, 1)
    start(UP, 0, (1,))
    for hop in range(2, hops):
        start(POOL, hop)
    share = pl.ds(core * (pool_full.shape[0] // cores), pool_full.shape[0] // cores)
    pool_full[share, pl.ds(pl.multiple_of(me_fs * depth, depth), depth), :] = pool_ref[share, :, :]
    mine = pl.ds(pl.multiple_of(me_fs * cols, cols), cols)
    up_full[:, mine] = up_ref[...]
    down_full[:, mine] = down_ref[...]
    for copy in halos:
        copy.wait()
    offset = me * rows
    lower_open = (lax.rem(offset, SEQ_LEN) != 0).astype(jnp.float32)
    upper_open = (lax.rem(offset + rows, SEQ_LEN) != 0).astype(jnp.float32)
    ext[0:HALO, :] = before[...].astype(jnp.float32) * lower_open
    ext[rows + HALO : rows + 2 * HALO, :] = after[...].astype(jnp.float32) * upper_open
    start(UP, 1)
    settle(POOL, hops - 2)
    finish(POOL)
    if cores > 1:
        swap = pltpu.make_async_remote_copy(
            src_ref=pool_full.at[share],
            dst_ref=pool_full.at[share],
            send_sem=pair_send,
            recv_sem=pair_recv,
            device_id={"fs": me_fs, "tp": me + 1 - 2 * core},
            device_id_type=MESH,
        )
        swap.start()
        other = pl.ds((1 - core) * (pool_full.shape[0] // cores), pool_full.shape[0] // cores)
        pltpu.make_async_remote_copy(
            src_ref=pool_full.at[other],
            dst_ref=pool_full.at[other],
            send_sem=pair_send,
            recv_sem=pair_recv,
            device_id={"fs": me_fs, "tp": me + 1 - 2 * core},
            device_id_type=MESH,
        ).wait_recv()

    position = lax.rem(offset + lax.broadcasted_iota(jnp.int32, (rows, 1), 0), SEQ_LEN)
    for index, reach in enumerate(WINDOWS):
        half = reach // 2
        c = slice(index * group, (index + 1) * group)
        level = ext[:, c]
        own = level[HALO : HALO + rows]
        shift = 1
        while shift < reach:
            level = level + pltpu.roll(level, shift, 0)
            shift *= 2
        if half > 1:
            level = pltpu.roll(level, rows + 2 * HALO - (half - 1), 0)
        window = level[HALO : HALO + rows]
        counts = (jnp.minimum(position + half, SEQ_LEN) - jnp.maximum(position - half, 0)).astype(jnp.float32)
        pooled = (window / counts - own).astype(jnp.bfloat16)
        mixed = jnp.dot(pooled, pool_full[index], preferred_element_type=jnp.float32)
        first[:, c] = (tok_ref[:, c].astype(jnp.float32) + mixed * scale_ref[:, c]).astype(jnp.bfloat16)
    for hop in range(2, 3):
        if hop < hops:
            start(UP, hop)

    @pl.loop(0, rows // step)
    def _(i):
        r = pl.ds(pl.multiple_of(i * step, step), step)
        x = first[r, :].astype(jnp.float32)
        y = x * lax.rsqrt(jnp.mean(x * x, axis=-1, keepdims=True) + EPS) * gmlp_ref[...]
        inner_all[pl.ds(pl.multiple_of(me * rows + i * step, step), step), :] = y.astype(jnp.bfloat16)

    my_rows = pl.ds(pl.multiple_of(me * rows, rows), rows)
    inners, firsts = [], []
    for d in range(1, tp):
        peer = lax.rem(me + d, tp)
        copy = pltpu.make_async_remote_copy(
            src_ref=inner_all.at[my_rows, :],
            dst_ref=inner_all.at[my_rows, :],
            send_sem=in_send.at[d],
            recv_sem=in_recv.at[d],
            device_id={"fs": me_fs, "tp": peer},
            device_id_type=MESH,
        )
        copy.start()
        inners.append(copy)
    for d in range(1, tp):
        peer = lax.rem(me + d, tp)
        copy = pltpu.make_async_remote_copy(
            src_ref=first.at[:, pl.ds(pl.multiple_of(peer * own_cols, own_cols), own_cols)],
            dst_ref=fcols.at[my_rows, :],
            send_sem=fc_send.at[d],
            recv_sem=fc_recv.at[d],
            device_id={"fs": me_fs, "tp": peer},
            device_id_type=MESH,
        )
        copy.start()
        firsts.append(copy)
    fcols[my_rows, :] = first[:, pl.ds(pl.multiple_of(me * own_cols, own_cols), own_cols)]

    for hop in range(3, hops):
        start(UP, hop)
    settle(UP, hops - 2)
    start(DOWN, 0)
    finish(UP)
    for d in range(1, tp):
        source = pl.ds(pl.multiple_of(lax.rem(me + tp - d, tp) * rows, rows), rows)
        pltpu.make_async_remote_copy(
            src_ref=inner_all.at[source, :],
            dst_ref=inner_all.at[source, :],
            send_sem=in_send.at[d],
            recv_sem=in_recv.at[d],
            device_id={"fs": me_fs, "tp": lax.rem(me + d, tp)},
            device_id_type=MESH,
        ).wait_recv()

    tile = min(256, hid)

    @pl.loop(0, hid // tile)
    def _(j):
        h = pl.ds(pl.multiple_of(j * tile, tile), tile)
        pre = lax.dot_general(
            inner_all[...], up_full[h, :], (((1,), (1,)), ((), ())), preferred_element_type=jnp.float32
        )
        hidden[:, h] = jnp.square(jnp.maximum(pre, 0.0)).astype(jnp.bfloat16)

    sums = []
    part = min(512, seq)

    def block(k, owner, sub):
        c = pl.ds(pl.multiple_of(owner * cols + sub * fine, fine), fine)

        @pl.loop(0, seq // part)
        def _(i):
            r = pl.ds(pl.multiple_of(i * part, part), part)
            blocks[k, sub, r, :] = jnp.dot(
                hidden[r, :], down_full[:, c], preferred_element_type=jnp.float32
            ).astype(jnp.bfloat16)

        dest = owner // per
        d = lax.rem(dest - me + tp, tp)
        local = lax.rem(owner, per)
        copy = pltpu.make_async_remote_copy(
            src_ref=blocks.at[k, sub],
            dst_ref=parts.at[d, local, sub],
            send_sem=rs_send.at[k * lanes + sub],
            recv_sem=rs_recv.at[(d * per + local) * lanes + sub],
            device_id={"fs": me_fs, "tp": dest},
            device_id_type=MESH,
        )

        @pl.when(d == 0)
        def _():
            parts[0, local, sub] = blocks[k, sub]

        @pl.when(d != 0)
        def _():
            copy.start()

        sums.append((d, copy))

    def add_up(local, sub):
        for d in range(1, tp):
            pltpu.make_async_remote_copy(
                src_ref=blocks.at[0, sub],
                dst_ref=parts.at[d, local, sub],
                send_sem=rs_send.at[0],
                recv_sem=rs_recv.at[(d * per + local) * lanes + sub],
                device_id={"fs": me_fs, "tp": lax.rem(me + d, tp)},
                device_id_type=MESH,
            ).wait_recv()
        c = pl.ds(pl.multiple_of(local * cols + sub * fine, fine), fine)

        @pl.loop(0, seq // 128)
        def _(i):
            r = pl.ds(pl.multiple_of(i * 128, 128), 128)
            value = parts[0, local, sub, r, :].astype(jnp.float32)
            for d in range(1, tp):
                value = value + parts[d, local, sub, r, :].astype(jnp.float32)
            value = value + fcols[r, c].astype(jnp.float32)
            total[r, c] = value
            square = value * value
            lump = square[:, 0:128]
            for j in range(1, fine // 128):
                lump = lump + square[:, j * 128 : (j + 1) * 128]
            stat[r, :] = stat[r, :] + lump

    for sub in range(lanes):
        block(0, owners[0], sub)
    stat[...] = jnp.zeros_like(stat)
    k = 1
    for hop in range(1, hops):
        start(DOWN, hop)
        settle(DOWN, hop - 1)
        for owner in (owners[-hop], owners[hop]):
            for sub in range(lanes):
                block(k, owner, sub)
            k += 1
    for copy in firsts:
        copy.wait()
    last = lax.rem(owners[hops], per)
    for j in range(1, per):
        for sub in range(lanes):
            add_up(lax.rem(last + j, per), sub)
    for sub in range(lanes):
        finish(DOWN, sub)
        block(k, owners[hops], sub)
    for sub in range(lanes):
        add_up(last, sub)

    turned = jnp.transpose(stat[...])
    stat_out[...] = jnp.broadcast_to(jnp.sum(turned, axis=0, keepdims=True), stat_out.shape)
    stats = []
    for d in range(1, tp):
        copy = pltpu.make_async_remote_copy(
            src_ref=stat_out,
            dst_ref=stat_in.at[d],
            send_sem=st_send.at[d],
            recv_sem=st_recv.at[d],
            device_id={"fs": me_fs, "tp": lax.rem(me + d, tp)},
            device_id_type=MESH,
        )
        copy.start()
        stats.append(copy)
    for copy in started:
        copy.wait_send()
    for copy in inners:
        copy.wait_send()
    if cores > 1:
        swap.wait_send()
    for d, copy in sums:
        @pl.when(d != 0)
        def _(copy=copy):
            copy.wait_send()
    for copy in stats:
        copy.wait()
    squares = stat_out[...]
    for d in range(1, tp):
        squares = squares + stat_in[d]
    factor = lax.rsqrt(squares / width + EPS)
    stat[...] = jnp.transpose(jnp.broadcast_to(factor[0:1], (128, seq)))

    @pl.loop(0, seq // 128)
    def _(i):
        r = pl.ds(pl.multiple_of(i * 128, 128), 128)
        out_ref[r, :] = (total[r, :] * stat[r, 0:1] * gout_ref[...]).astype(jnp.bfloat16)


def local(order, tokens, pool_weight, pool_scale, gain_mix, gain_mlp, w_up, w_down, gain_out):
    n, tp = lax.axis_size("fs"), lax.axis_size("tp")
    rows, width = tokens.shape
    hid, cols = w_up.shape
    seq, own = rows * tp, width // tp
    bf, f32 = jnp.bfloat16, jnp.float32
    vmem = pl.BlockSpec(memory_space=pltpu.VMEM)
    dma = pltpu.SemaphoreType.DMA
    lanes = 2 if cols % 256 == 0 else 1
    return pl.pallas_call(
        functools.partial(kernel, n, tp, order),
        out_shape=jax.ShapeDtypeStruct((seq, own), bf),
        in_specs=[vmem] * 8,
        out_specs=vmem,
        scratch_shapes=[
            pltpu.VMEM((pool_weight.shape[0], pool_weight.shape[1] * n, pool_weight.shape[2]), bf),
            pltpu.VMEM((hid, width), bf),
            pltpu.VMEM((hid, width), bf),
            pltpu.VMEM((rows + 2 * HALO, width), f32),
            pltpu.VMEM((rows, width), bf),
            pltpu.VMEM((seq, width), bf),
            pltpu.VMEM((seq, hid), bf),
            pltpu.VMEM((seq, own), bf),
            pltpu.VMEM((n, lanes, seq, cols // lanes), bf),
            pltpu.VMEM((tp, n // tp, lanes, seq, cols // lanes), bf),
            pltpu.VMEM((HALO, width), bf),
            pltpu.VMEM((HALO, width), bf),
            pltpu.VMEM((2, HALO, width), bf),
            pltpu.VMEM((seq, own), f32),
            pltpu.VMEM((seq, 128), f32),
            pltpu.VMEM((8, seq), f32),
            pltpu.VMEM((tp, 8, seq), f32),
            dma((12 * (n // 2) + 2 * lanes,)),
            dma((12 * (n // 2) + 2 * lanes,)),
            dma((tp,)),
            dma((tp,)),
            dma((tp,)),
            dma((tp,)),
            dma((2,)),
            dma((2,)),
            dma((n * lanes,)),
            dma((n * lanes,)),
            dma,
            dma,
            dma((tp,)),
            dma((tp,)),
        ],
        compiler_params=pltpu.CompilerParams(
            collective_id=0, has_side_effects=True, vmem_limit_bytes=63 * 1024 * 1024
        ),
    )(
        tokens, pool_weight, w_up, w_down,
        pool_scale.reshape(1, -1), gain_mix.reshape(1, -1), gain_mlp.reshape(1, -1),
        gain_out.reshape(1, -1),
    )


def grid_width(mesh):
    n = mesh.shape["fs"]
    try:
        line = mesh.devices.reshape(n, -1)[:, 0]
        nx = len({d.coords[0] for d in line})
        if n % nx == 0:
            return nx
    except AttributeError:
        pass
    return 2 if n % 2 == 0 else 1


def solution(mesh):
    order = ring_order(mesh.shape["fs"], grid_width(mesh))
    return jax.shard_map(
        functools.partial(local, order),
        mesh=mesh,
        in_specs=(
            P(("fs", "tp"), None),
            P(None, "fs", None),
            P(),
            P(),
            P(),
            P("tp", "fs"),
            P("tp", "fs"),
            P("tp"),
        ),
        out_specs=P("fs", "tp"),
        check_vma=False,
    )
```

profile of v0, /device:TPU:0, one launch (start us, length us, event | category | flops | bytes accessed | tf_op | source)
XLA Modules:
  0.0 203.2 jit_solution(11824925044379597436)
XLA Ops:
  0.0 200.9 %shard_map.82 = bf16[1024,512]{1,0:T(8,128)(2,1)} custom-call(bf16[256,2048]{1,0:T(8,128)(2,1)} %tok_ref.1, bf16[4,64,512]{2,1,0:T(8,128)(2,1)} %pool_ref.1, bf16[2048,256]{1,0:T(8,128)(2,1)} %up_ref.1, bf16[2048,256]{1,0:T(8,128)(2,1)} %down_ref.1, f32[1,2048]{1,0:T(1,128)} %bitcast.4, f32[1,2048]{1,0:T(1,128)} %bitcast.5, f32[1,2048]{1,0:T(1,128)} %bitcast.6, ...), custom_call_target="tpu_custom_call" | custom-call | tf_op jit(solution)/shard_map/pallas_call | solution.py:428
  200.9 2.3 %copy.10 = bf16[1024,512]{1,0:T(8,128)(2,1)} copy(bf16[1024,512]{1,0:T(8,128)(2,1)} %shard_map.82) | data formatting | bytes 2097152
where the time goes:
time: 205 us; the launch traced here: 203 us
  Pallas kernels  201 us (98%)
  local copies, waits for them, and re-layouts  2.26 us (1%)
    pallas_call x1, Pallas kernels, local(): pl.pallas_call(functools.partial(kernel, n, tp, order), out_shape=jax.Sha...  201 us

commit v1 on v0

--- a/solution.py
+++ b/solution.py
@@ -33,7 +33,7 @@
     return value
 
 
-def kernel(
+def ring_kernel(
     n, tp, order, tok_ref, pool_ref, up_ref, down_ref, scale_ref, gmix_ref, gmlp_ref,
     gout_ref, out_ref,
     pool_full, up_full, down_full, ext, first, inner_all, hidden, fcols, blocks, parts,
@@ -416,7 +416,7 @@
         out_ref[r, :] = (total[r, :] * stat[r, 0:1] * gout_ref[...]).astype(jnp.bfloat16)
 
 
-def local(order, tokens, pool_weight, pool_scale, gain_mix, gain_mlp, w_up, w_down, gain_out):
+def ring_local(order, tokens, pool_weight, pool_scale, gain_mix, gain_mlp, w_up, w_down, gain_out):
     n, tp = lax.axis_size("fs"), lax.axis_size("tp")
     rows, width = tokens.shape
     hid, cols = w_up.shape
@@ -426,7 +426,7 @@
     dma = pltpu.SemaphoreType.DMA
     lanes = 2 if cols % 256 == 0 else 1
     return pl.pallas_call(
-        functools.partial(kernel, n, tp, order),
+        functools.partial(ring_kernel, n, tp, order),
         out_shape=jax.ShapeDtypeStruct((seq, own), bf),
         in_specs=[vmem] * 8,
         out_specs=vmem,
@@ -473,6 +473,496 @@
     )
 
 
+NEAR = ((1, 2, 3), (0, 2, 3), (3, 1, 0), (2, 1, 0))
+TARGETS = ((1, 2, 3), (0, 3, 2), (3, 0, 1), (2, 1, 0))
+Y_FIRST = (True, False, True, False)
+ENDS, INNER = 4, 4
+UPS, DOWNS = 0, 1
+
+
+def plane_kernel(
+    tok_ref, pool_ref, up_ref, down_ref, scale_ref, gmix_ref, gmlp_ref, gout_ref, out_ref,
+    pool_full, up_full, down_full, ext, first_all, inner, hidden,
+    part_send, part_recv, part, y_recv, z_recv,
+    before, after, edge, total, stat, stat_out, stat_in,
+    pz_s, pz_r, px_s, px_r, swap_s, swap_r, wz_s, wz_r, wx_s, wx_r, halo_s, halo_r,
+    f_s, f_r, d_s, d_r, y_s, y_r, z_s, z_r, st_s, st_r,
+):
+    rows, width = tok_ref.shape
+    group = width // 4
+    hid, cols = up_ref.shape
+    depth = pool_ref.shape[1]
+    nz, tp = 4, 4
+    own_cols = width // tp
+    seq = rows * tp
+    most = max(ENDS, INNER)
+    piece = hid // (ENDS + INNER)
+    bf, f32 = jnp.bfloat16, jnp.float32
+    me_fs, me = lax.axis_index("fs"), lax.axis_index("tp")
+    z, x = lax.div(me_fs, 2), lax.rem(me_fs, 2)
+    y, c = lax.div(me, 2), lax.rem(me, 2)
+    q = lax.rem(z, 2)
+    zp = z + 1 - 2 * q
+
+    def pick(table, column):
+        return lookup([row[column] for row in table], z)
+
+    def is_end(plane):
+        return (plane == 0) | (plane == nz - 1)
+
+    def count_of(plane):
+        return jnp.where(is_end(plane), ENDS, INNER)
+
+    def base_of(plane):
+        return jnp.where(is_end(plane), 0, ENDS * piece)
+
+    def dev(z=z, x=x, y=y, c=c):
+        return {"fs": z * 2 + x, "tp": y * 2 + c}
+
+    def rc(src, dst, send, recv, to):
+        return pltpu.make_async_remote_copy(
+            src_ref=src, dst_ref=dst, send_sem=send, recv_sem=recv, device_id=to, device_id_type=MESH
+        )
+
+    def landed(dst, recv):
+        pltpu.make_async_remote_copy(
+            src_ref=dst, dst_ref=dst, send_sem=recv, recv_sem=recv, device_id=dev(x=1 - x), device_id_type=MESH
+        ).wait_recv()
+
+    barrier = pltpu.get_barrier_semaphore()
+    peers = [dev(z=pick(TARGETS, k)) for k in range(3)] + [dev(x=1 - x), dev(y=1 - y), dev(c=1 - c)]
+    peers.append(dev(y=1 - y, c=1 - c))
+    for peer in peers:
+        pl.semaphore_signal(barrier, inc=1, device_id=peer, device_id_type=MESH)
+    pl.semaphore_wait(barrier, len(peers))
+
+    always, pending = None, []
+
+    def go(copy, condition=always):
+        if condition is None:
+            copy.start()
+        else:
+            @pl.when(condition)
+            def _():
+                copy.start()
+        pending.append((copy, condition))
+
+    gpc = pool_ref.shape[0] // 2
+    mine_groups = pl.ds(c * gpc, gpc)
+
+    def pool_block(plane, column):
+        return pool_full.at[mine_groups, pl.ds(pl.multiple_of((plane * 2 + column) * depth, depth), depth), :]
+
+    own_pool = pool_ref.at[mine_groups]
+    for k in range(3):
+        t = pick(TARGETS, k)
+        go(rc(own_pool, pool_block(z, x), pz_s.at[t], pz_r.at[z], dev(z=t)))
+    go(rc(own_pool, pool_block(z, x), px_s.at[z], px_r.at[z], dev(x=1 - x)))
+
+    weights = (up_ref, down_ref)
+    fulls = (up_full, down_full)
+
+    def slot(stream, plane, p):
+        return (stream * nz + plane) * most + p
+
+    def block(stream, plane, column, p):
+        return fulls[stream].at[
+            pl.ds(p * piece, piece), pl.ds(pl.multiple_of((plane * 2 + column) * cols, cols), cols)
+        ]
+
+    def own_piece(stream, plane, p):
+        start = pl.multiple_of(base_of(plane) + p * piece, piece)
+        return weights[stream].at[pl.ds(start, piece), :]
+
+    def some(p, plane):
+        return always if p < min(ENDS, INNER) else p < count_of(plane)
+
+    def spread_z(stream):
+        for k in range(3):
+            t = pick(TARGETS, k)
+            for p in range(most):
+                go(
+                    rc(own_piece(stream, t, p), block(stream, z, x, p), wz_s.at[slot(stream, t, p)],
+                       wz_r.at[slot(stream, z, p)], dev(z=t)),
+                    some(p, t),
+                )
+
+    def spread_x(stream):
+        for p in range(most):
+            go(
+                rc(own_piece(stream, z, p), block(stream, z, x, p), wx_s.at[slot(stream, z, p)],
+                   wx_r.at[slot(stream, z, p)], dev(x=1 - x)),
+                some(p, z),
+            )
+
+    def guarded(condition, body):
+        if condition is None:
+            body()
+        else:
+            pl.when(condition)(body)
+
+    def relay(stream, k):
+        s = pick(NEAR, k)
+        for p in range(most):
+            condition = some(p, z)
+            ref = block(stream, s, x, p)
+            guarded(condition, lambda ref=ref, p=p: landed(ref, wz_r.at[slot(stream, s, p)]))
+            go(rc(ref, ref, wx_s.at[slot(stream, s, p)], wx_r.at[slot(stream, s, p)], dev(x=1 - x)), condition)
+
+    def from_x(stream, s):
+        for p in range(most):
+            ref = block(stream, s, 1 - x, p)
+            guarded(some(p, z), lambda ref=ref, p=p: landed(ref, wx_r.at[slot(stream, s, p)]))
+
+    spread_z(UPS)
+    spread_x(UPS)
+
+    step = 32 if rows % 32 == 0 else rows
+
+    @pl.loop(0, rows // step)
+    def _(i):
+        r = pl.ds(pl.multiple_of(i * step, step), step)
+        v = tok_ref[r, :].astype(f32)
+        v = v * lax.rsqrt(jnp.mean(v * v, axis=-1, keepdims=True) + EPS) * gmix_ref[...]
+        v = v.astype(bf)
+        ext[pl.ds(pl.multiple_of(HALO + i * step, HALO), step), :] = v.astype(f32)
+
+    edge[0] = ext[rows : rows + HALO, :].astype(bf)
+    edge[1] = ext[HALO : 2 * HALO, :].astype(bf)
+    for side, (buffer, d) in enumerate(((before, 1), (after, tp - 1))):
+        to = {"fs": me_fs, "tp": lax.rem(me + d, tp)}
+        go(rc(edge.at[side], buffer, halo_s.at[side], halo_r.at[side], to))
+
+    pool_full[mine_groups, pl.ds(pl.multiple_of(me_fs * depth, depth), depth), :] = pool_ref[mine_groups, :, :]
+    for k in range(3):
+        s = pick(NEAR, k)
+        ref = pool_block(s, x)
+        landed(ref, pz_r.at[s])
+        go(rc(ref, ref, px_s.at[s], px_r.at[s], dev(x=1 - x)))
+    mine = pl.ds(pl.multiple_of(me_fs * cols, cols), cols)
+    for stream in (UPS, DOWNS):
+        for p in range(most):
+            def keep(stream=stream, p=p):
+                start = pl.multiple_of(base_of(z) + p * piece, piece)
+                fulls[stream][p * piece : (p + 1) * piece, mine] = weights[stream][pl.ds(start, piece), :]
+            guarded(some(p, z), keep)
+    landed(before, halo_r.at[0])
+    landed(after, halo_r.at[1])
+    offset = me * rows
+    lower_open = (lax.rem(offset, SEQ_LEN) != 0).astype(f32)
+    upper_open = (lax.rem(offset + rows, SEQ_LEN) != 0).astype(f32)
+    ext[0:HALO, :] = before[...].astype(f32) * lower_open
+    ext[rows + HALO : rows + 2 * HALO, :] = after[...].astype(f32) * upper_open
+    for s in range(nz):
+        landed(pool_block(s, 1 - x), px_r.at[s])
+    go(rc(pool_full.at[mine_groups], pool_full.at[mine_groups], swap_s, swap_r, dev(c=1 - c)))
+    landed(pool_full.at[pl.ds((1 - c) * gpc, gpc)], swap_r)
+
+    def rows_of(s, t):
+        return pl.ds(pl.multiple_of(s * seq + t * rows, rows), rows)
+
+    my_rows = rows_of(q, me)
+    position = lax.rem(offset + lax.broadcasted_iota(jnp.int32, (rows, 1), 0), SEQ_LEN)
+    for index, reach in enumerate(WINDOWS):
+        half = reach // 2
+        g = slice(index * group, (index + 1) * group)
+        level = ext[:, g]
+        own = level[HALO : HALO + rows]
+        shift = 1
+        while shift < reach:
+            level = level + pltpu.roll(level, shift, 0)
+            shift *= 2
+        if half > 1:
+            level = pltpu.roll(level, rows + 2 * HALO - (half - 1), 0)
+        window = level[HALO : HALO + rows]
+        counts = (jnp.minimum(position + half, SEQ_LEN) - jnp.maximum(position - half, 0)).astype(f32)
+        pooled = (window / counts - own).astype(bf)
+        mixed = jnp.dot(pooled, pool_full[index], preferred_element_type=f32)
+        first_all[my_rows, g] = (tok_ref[:, g].astype(f32) + mixed * scale_ref[:, g]).astype(bf)
+
+    def share(s, t, k, to):
+        ref = first_all.at[rows_of(s, t), :]
+        go(rc(ref, ref, f_s.at[k], f_r.at[k], to))
+
+    def shared(s, t, k):
+        landed(first_all.at[rows_of(s, t), :], f_r.at[k])
+
+    peer_y, peer_c = (1 - y) * 2 + c, y * 2 + 1 - c
+    peer_yc = (1 - y) * 2 + 1 - c
+    share(q, me, 0, dev(z=zp))
+    share(q, me, 1, dev(y=1 - y))
+    share(q, me, 3, dev(c=1 - c))
+    spread_z(DOWNS)
+    spread_x(DOWNS)
+    for k in range(3):
+        relay(UPS, k)
+
+    def norm_up(s, yy):
+        begin = s * seq + yy * 2 * rows
+
+        @pl.loop(0, 2 * rows // step)
+        def _(i):
+            r = pl.ds(pl.multiple_of(begin + i * step, step), step)
+            v = first_all[r, :].astype(f32)
+            v = v * lax.rsqrt(jnp.mean(v * v, axis=-1, keepdims=True) + EPS) * gmlp_ref[...]
+            inner[pl.ds(pl.multiple_of(i * step, step), step), :] = v.astype(bf)
+
+        @pl.loop(0, count_of(z))
+        def _(j):
+            h = pl.ds(pl.multiple_of(j * piece, piece), piece)
+            pre = lax.dot_general(
+                inner[...], up_full[h, :], (((1,), (1,)), ((), ())), preferred_element_type=f32
+            )
+            hidden[pl.ds(pl.multiple_of(begin, 2 * rows), 2 * rows), h] = jnp.square(jnp.maximum(pre, 0.0)).astype(bf)
+
+    shared(1 - q, me, 0)
+    share(1 - q, me, 2, dev(y=1 - y))
+    share(1 - q, me, 4, dev(c=1 - c))
+    for s in range(nz):
+        from_x(UPS, s)
+    shared(q, peer_c, 3)
+    norm_up(q, y)
+    shared(q, peer_y, 1)
+    share(q, peer_y, 5, dev(c=1 - c))
+    shared(1 - q, peer_c, 4)
+    norm_up(1 - q, y)
+    relay(DOWNS, 0)
+    shared(q, peer_yc, 5)
+    norm_up(q, 1 - y)
+    relay(DOWNS, 1)
+    shared(1 - q, peer_y, 2)
+    share(1 - q, peer_y, 6, dev(c=1 - c))
+    shared(1 - q, peer_yc, 6)
+    norm_up(1 - q, 1 - y)
+
+    chunk = 2 * rows
+    orow = pl.ds(pl.multiple_of(q * seq, seq), seq)
+    prow = pl.ds(pl.multiple_of((1 - q) * seq, seq), seq)
+    fine = 128
+
+    def unit(i, j):
+        plane = jnp.where(z < 2, i, nz - 1 - i)
+        column = x if j == 0 else 1 - x
+        return plane, column, (i // 2) * 2 + j, i * 2 + j
+
+    def each(begin, size, body):
+        @pl.loop(0, size // fine)
+        def _(i):
+            body(pl.ds(pl.multiple_of(begin + i * fine, fine), fine), pl.ds(pl.multiple_of(i * fine, fine), fine))
+
+    def product(i, j):
+        plane, column, s, u = unit(i, j)
+        cc = pl.ds(pl.multiple_of((plane * 2 + column) * cols, cols), cols)
+        theirs = lax.rem(plane, 2) != c
+        if j == 1:
+            from_x(DOWNS, plane)
+
+        def all_rows(depth_of):
+            @pl.loop(0, 2 * seq // chunk)
+            def _(k):
+                r = pl.ds(pl.multiple_of(k * chunk, chunk), chunk)
+                value = jnp.dot(hidden[r, 0:depth_of], down_full[0:depth_of, cc], preferred_element_type=f32)
+
+                @pl.when(theirs)
+                def _():
+                    part_send[s, r, :] = value.astype(bf)
+
+                @pl.when(jnp.logical_not(theirs))
+                def _():
+                    part[s, r, :] = value
+
+        if ENDS == INNER:
+            all_rows(ENDS * piece)
+        else:
+            pl.when(is_end(z))(lambda: all_rows(ENDS * piece))
+            pl.when(jnp.logical_not(is_end(z)))(lambda: all_rows(INNER * piece))
+        go(rc(part_send.at[s], part_recv.at[s], d_s.at[u], d_r.at[u], dev(c=1 - c)), theirs)
+
+    def stage1(i, j):
+        plane, column, s, u = unit(i, j)
+        ours = lax.rem(plane, 2) == c
+        home = lax.div(plane, 2) == y
+
+        def fold(begin, size, keep):
+            def body(r, _):
+                value = part[s, r, :] + part_recv[s, r, :].astype(f32)
+                if keep:
+                    part[s, r, :] = value
+                else:
+                    part_recv[s, r, :] = value.astype(bf)
+            each(begin, size, body)
+
+        @pl.when(ours)
+        def _():
+            landed(part_recv.at[s], d_r.at[u])
+            if not Y_FIRST[i]:
+                fold((1 - q) * seq, seq, False)
+
+        if Y_FIRST[i]:
+            pl.when(ours & home)(lambda: fold(0, 2 * seq, True))
+            pl.when(ours & jnp.logical_not(home))(lambda: fold(0, 2 * seq, False))
+            go(rc(part_recv.at[s], y_recv.at[j], y_s.at[u], y_r.at[u], dev(y=1 - y)), ours & jnp.logical_not(home))
+        else:
+            go(rc(part_recv.at[s, prow, :], z_recv.at[s], z_s.at[u], z_r.at[u], dev(z=zp)), ours)
+            pl.when(ours)(lambda: fold(q * seq, seq, True))
+
+    def stage2(i, j):
+        plane, column, s, u = unit(i, j)
+        ours = lax.rem(plane, 2) == c
+        home = lax.div(plane, 2) == y
+        if Y_FIRST[i]:
+            @pl.when(ours & home)
+            def _():
+                landed(y_recv.at[j], y_r.at[u])
+
+                def out(r, _):
+                    y_recv[j, r, :] = (part[s, r, :] + y_recv[j, r, :].astype(f32)).astype(bf)
+                each((1 - q) * seq, seq, out)
+
+            go(rc(y_recv.at[j, prow, :], z_recv.at[s], z_s.at[u], z_r.at[u], dev(z=zp)), ours & home)
+
+            @pl.when(ours & home)
+            def _():
+                def kept(r, _):
+                    part[s, r, :] = part[s, r, :] + y_recv[j, r, :].astype(f32)
+                each(q * seq, seq, kept)
+        else:
+            @pl.when(ours)
+            def _():
+                landed(z_recv.at[s], z_r.at[u])
+
+            @pl.when(ours & jnp.logical_not(home))
+            def _():
+                def out(r, l):
+                    part_recv[s, r, :] = (part[s, r, :] + z_recv[s, l, :].astype(f32)).astype(bf)
+                each(q * seq, seq, out)
+
+            go(rc(part_recv.at[s, orow, :], y_recv.at[j, orow, :], y_s.at[u], y_r.at[u], dev(y=1 - y)),
+               ours & jnp.logical_not(home))
+
+            @pl.when(ours & home)
+            def _():
+                def kept(r, l):
+                    part[s, r, :] = part[s, r, :] + z_recv[s, l, :].astype(f32)
+                each(q * seq, seq, kept)
+
+    def stage3(i, j):
+        plane, column, s, u = unit(i, j)
+
+        @pl.when(plane == me)
+        def _():
+            if Y_FIRST[i]:
+                landed(z_recv.at[s], z_r.at[u])
+            else:
+                landed(y_recv.at[j, orow, :], y_r.at[u])
+            here = pl.ds(pl.multiple_of(column * cols, cols), cols)
+            cc = pl.ds(pl.multiple_of(me * own_cols + column * cols, cols), cols)
+
+            def body(r, l):
+                more = z_recv[s, l, :] if Y_FIRST[i] else y_recv[j, r, :]
+                value = part[s, r, :] + more.astype(f32) + first_all[r, cc].astype(f32)
+                total[l, here] = value
+                square = value * value
+                lump = square[:, 0:128]
+                for k in range(1, cols // 128):
+                    lump = lump + square[:, k * 128 : (k + 1) * 128]
+                stat[l, :] = stat[l, :] + lump
+            each(q * seq, seq, body)
+
+    stat[...] = jnp.zeros_like(stat)
+    both = (0, 1)
+
+    def run(body, i):
+        for j in both:
+            body(i, j)
+
+    for i in range(3):
+        run(product, i)
+        run(stage1, i)
+    for i in range(3):
+        run(stage2, i)
+    relay(DOWNS, 2)
+    run(product, 3)
+    run(stage1, 3)
+    run(stage3, 0)
+    run(stage3, 1)
+    run(stage2, 3)
+    run(stage3, 2)
+    run(stage3, 3)
+
+    turned = jnp.transpose(stat[...])
+    stat_out[...] = jnp.broadcast_to(jnp.sum(turned, axis=0, keepdims=True), stat_out.shape)
+    for d in range(1, tp):
+        to = {"fs": me_fs, "tp": lax.rem(me + d, tp)}
+        go(rc(stat_out, stat_in.at[d], st_s.at[d], st_r.at[d], to))
+    for copy, condition in pending:
+        guarded(condition, copy.wait_send)
+    squares = stat_out[...]
+    for d in range(1, tp):
+        landed(stat_in.at[d], st_r.at[d])
+        squares = squares + stat_in[d]
+    factor = lax.rsqrt(squares / width + EPS)
+    stat[...] = jnp.transpose(jnp.broadcast_to(factor[0:1], (128, seq)))
+
+    @pl.loop(0, seq // 128)
+    def _(i):
+        r = pl.ds(pl.multiple_of(i * 128, 128), 128)
+        out_ref[r, :] = (total[r, :] * stat[r, 0:1] * gout_ref[...]).astype(bf)
+
+
+def plane_local(tokens, pool_weight, pool_scale, gain_mix, gain_mlp, w_up, w_down, gain_out):
+    n, tp = lax.axis_size("fs"), lax.axis_size("tp")
+    rows, width = tokens.shape
+    hid, cols = w_up.shape
+    seq, own = rows * tp, width // tp
+    bf, f32 = jnp.bfloat16, jnp.float32
+    vmem = pl.BlockSpec(memory_space=pltpu.VMEM)
+    dma = pltpu.SemaphoreType.DMA
+    most = max(ENDS, INNER)
+    deep = hid // (ENDS + INNER) * most
+    lots = 2 * 4 * most
+    return pl.pallas_call(
+        plane_kernel,
+        out_shape=jax.ShapeDtypeStruct((seq, own), bf),
+        in_specs=[vmem] * 8,
+        out_specs=vmem,
+        scratch_shapes=[
+            pltpu.VMEM((pool_weight.shape[0], pool_weight.shape[1] * n, pool_weight.shape[2]), bf),
+            pltpu.VMEM((deep, width), bf),
+            pltpu.VMEM((deep, width), bf),
+            pltpu.VMEM((rows + 2 * HALO, width), f32),
+            pltpu.VMEM((2 * seq, width), bf),
+            pltpu.VMEM((2 * rows, width), bf),
+            pltpu.VMEM((2 * seq, deep), bf),
+            pltpu.VMEM((4, 2 * seq, cols), bf),
+            pltpu.VMEM((4, 2 * seq, cols), bf),
+            pltpu.VMEM((4, 2 * seq, cols), f32),
+            pltpu.VMEM((2, 2 * seq, cols), bf),
+            pltpu.VMEM((4, seq, cols), bf),
+            pltpu.VMEM((HALO, width), bf),
+            pltpu.VMEM((HALO, width), bf),
+            pltpu.VMEM((2, HALO, width), bf),
+            pltpu.VMEM((seq, own), f32),
+            pltpu.VMEM((seq, 128), f32),
+            pltpu.VMEM((8, seq), f32),
+            pltpu.VMEM((tp, 8, seq), f32),
+            dma((4,)), dma((4,)), dma((4,)), dma((4,)), dma, dma,
+            dma((lots,)), dma((lots,)), dma((lots,)), dma((lots,)),
+            dma((2,)), dma((2,)),
+            dma((7,)), dma((7,)),
+            dma((8,)), dma((8,)), dma((8,)), dma((8,)), dma((8,)), dma((8,)),
+            dma((tp,)), dma((tp,)),
+        ],
+        compiler_params=pltpu.CompilerParams(
+            collective_id=0, has_side_effects=True, vmem_limit_bytes=63 * 1024 * 1024
+        ),
+    )(
+        tokens, pool_weight, w_up, w_down,
+        pool_scale.reshape(1, -1), gain_mix.reshape(1, -1), gain_mlp.reshape(1, -1),
+        gain_out.reshape(1, -1),
+    )
+
+
 def grid_width(mesh):
     n = mesh.shape["fs"]
     try:
@@ -486,9 +976,13 @@
 
 
 def solution(mesh):
-    order = ring_order(mesh.shape["fs"], grid_width(mesh))
+    n, tp, nx = mesh.shape["fs"], mesh.shape["tp"], grid_width(mesh)
+    if nx == 2 and n == 8 and tp == 4:
+        body = plane_local
+    else:
+        body = functools.partial(ring_local, ring_order(n, nx))
     return jax.shard_map(
-        functools.partial(local, order),
+        body,
         mesh=mesh,
         in_specs=(
             P(("fs", "tp"), None),

time: 205 us -> 194 us (0.946)
  Pallas kernels: 201 us -> 192 us
    pallas_call x1, Pallas kernels: 201 us -> 192 us  [plane_local(): pl.pallas_call(plane_kernel, out_shape=jax.ShapeDtypeStruct((seq, own), b...]
where the time goes in v1:
time: 194 us
  Pallas kernels  192 us (99%)
  local copies, waits for them, and re-layouts  2.26 us (1%)
    pallas_call x1, Pallas kernels, plane_local(): pl.pallas_call(plane_kernel, out_shape=jax.ShapeDtypeStruct((seq, own), b...  192 us

profile of v1, /device:TPU:0, one launch (start us, length us, event | category | flops | bytes accessed | tf_op | source)
XLA Modules:
  0.0 194.2 jit_solution(3797838784703250601)
XLA Ops:
  0.0 192.0 %shard_map.82 = bf16[1024,512]{1,0:T(8,128)(2,1)} custom-call(bf16[256,2048]{1,0:T(8,128)(2,1)} %tok_ref.1, bf16[4,64,512]{2,1,0:T(8,128)(2,1)} %pool_ref.1, bf16[2048,256]{1,0:T(8,128)(2,1)} %up_ref.1, bf16[2048,256]{1,0:T(8,128)(2,1)} %down_ref.1, f32[1,2048]{1,0:T(1,128)} %bitcast.4, f32[1,2048]{1,0:T(1,128)} %bitcast.5, f32[1,2048]{1,0:T(1,128)} %bitcast.6, ...), custom_call_target="tpu_custom_call" | custom-call | tf_op jit(solution)/shard_map/pallas_call | solution.py:924
  192.0 2.3 %copy.10 = bf16[1024,512]{1,0:T(8,128)(2,1)} copy(bf16[1024,512]{1,0:T(8,128)(2,1)} %shard_map.82) | data formatting | bytes 2097152

commit v2 on v1

--- a/solution.py
+++ b/solution.py
@@ -478,14 +478,15 @@
 Y_FIRST = (True, False, True, False)
 ENDS, INNER = 4, 4
 UPS, DOWNS = 0, 1
+HALVES = 2
 
 
 def plane_kernel(
     tok_ref, pool_ref, up_ref, down_ref, scale_ref, gmix_ref, gmlp_ref, gout_ref, out_ref,
-    pool_full, up_full, down_full, ext, first_all, inner, hidden,
+    pool_full, up_full, down_full, ext, first_all, inner_all, hidden,
     part_send, part_recv, part, y_recv, z_recv,
     before, after, edge, total, stat, stat_out, stat_in,
-    pz_s, pz_r, px_s, px_r, swap_s, swap_r, wz_s, wz_r, wx_s, wx_r, halo_s, halo_r,
+    pz_s, pz_r, px_s, px_r, py_s, py_r, pc_s, pc_r, wz_s, wz_r, wx_s, wx_r, halo_s, halo_r,
     f_s, f_r, d_s, d_r, y_s, y_r, z_s, z_r, st_s, st_r,
 ):
     rows, width = tok_ref.shape
@@ -547,17 +548,25 @@
                 copy.start()
         pending.append((copy, condition))
 
-    gpc = pool_ref.shape[0] // 2
-    mine_groups = pl.ds(c * gpc, gpc)
-
-    def pool_block(plane, column):
-        return pool_full.at[mine_groups, pl.ds(pl.multiple_of((plane * 2 + column) * depth, depth), depth), :]
-
-    own_pool = pool_ref.at[mine_groups]
+    def pool_block(g, plane, column):
+        return pool_full.at[g, pl.ds(pl.multiple_of((plane * 2 + column) * depth, depth), depth), :]
+
+    def pool_to_y(ref, plane, column):
+        f = plane * 2 + column
+        go(rc(ref, pool_block(me, plane, column), py_s.at[f], py_r.at[f], dev(y=1 - y)))
+
+    def pool_to_x(ref, plane):
+        go(rc(ref, pool_block(me, plane, x), px_s.at[plane], px_r.at[plane], dev(x=1 - x)))
+
+    def pool_to_c(g, k):
+        go(rc(pool_full.at[g], pool_full.at[g], pc_s.at[k], pc_r.at[k], dev(c=1 - c)))
+
+    own_pool = pool_ref.at[me]
     for k in range(3):
         t = pick(TARGETS, k)
-        go(rc(own_pool, pool_block(z, x), pz_s.at[t], pz_r.at[z], dev(z=t)))
-    go(rc(own_pool, pool_block(z, x), px_s.at[z], px_r.at[z], dev(x=1 - x)))
+        go(rc(own_pool, pool_block(me, z, x), pz_s.at[t], pz_r.at[z], dev(z=t)))
+    pool_to_x(own_pool, z)
+    pool_to_y(own_pool, z, x)
 
     weights = (up_ref, down_ref)
     fulls = (up_full, down_full)
@@ -577,18 +586,17 @@
     def some(p, plane):
         return always if p < min(ENDS, INNER) else p < count_of(plane)
 
-    def spread_z(stream):
-        for k in range(3):
+    def spread_z(stream, order):
+        for p, k in order:
             t = pick(TARGETS, k)
-            for p in range(most):
-                go(
-                    rc(own_piece(stream, t, p), block(stream, z, x, p), wz_s.at[slot(stream, t, p)],
-                       wz_r.at[slot(stream, z, p)], dev(z=t)),
-                    some(p, t),
-                )
-
-    def spread_x(stream):
-        for p in range(most):
+            go(
+                rc(own_piece(stream, t, p), block(stream, z, x, p), wz_s.at[slot(stream, t, p)],
+                   wz_r.at[slot(stream, z, p)], dev(z=t)),
+                some(p, t),
+            )
+
+    def spread_x(stream, pieces):
+        for p in pieces:
             go(
                 rc(own_piece(stream, z, p), block(stream, z, x, p), wx_s.at[slot(stream, z, p)],
                    wx_r.at[slot(stream, z, p)], dev(x=1 - x)),
@@ -601,21 +609,24 @@
         else:
             pl.when(condition)(body)
 
-    def relay(stream, k):
+    def relay(stream, k, pieces):
         s = pick(NEAR, k)
-        for p in range(most):
+        for p in pieces:
             condition = some(p, z)
             ref = block(stream, s, x, p)
             guarded(condition, lambda ref=ref, p=p: landed(ref, wz_r.at[slot(stream, s, p)]))
             go(rc(ref, ref, wx_s.at[slot(stream, s, p)], wx_r.at[slot(stream, s, p)], dev(x=1 - x)), condition)
 
-    def from_x(stream, s):
-        for p in range(most):
+    def from_x(stream, s, pieces):
+        for p in pieces:
             ref = block(stream, s, 1 - x, p)
             guarded(some(p, z), lambda ref=ref, p=p: landed(ref, wx_r.at[slot(stream, s, p)]))
 
-    spread_z(UPS)
-    spread_x(UPS)
+    every = range(most)
+    early = range(most // 2)
+    late = range(most // 2, most)
+    spread_z(UPS, [(p, k) for p in every for k in range(3)])
+    spread_x(UPS, early)
 
     step = 32 if rows % 32 == 0 else rows
 
@@ -633,12 +644,14 @@
         to = {"fs": me_fs, "tp": lax.rem(me + d, tp)}
         go(rc(edge.at[side], buffer, halo_s.at[side], halo_r.at[side], to))
 
-    pool_full[mine_groups, pl.ds(pl.multiple_of(me_fs * depth, depth), depth), :] = pool_ref[mine_groups, :, :]
+    pool_full[me, pl.ds(pl.multiple_of(me_fs * depth, depth), depth), :] = pool_ref[me, :, :]
     for k in range(3):
         s = pick(NEAR, k)
-        ref = pool_block(s, x)
+        ref = pool_block(me, s, x)
         landed(ref, pz_r.at[s])
-        go(rc(ref, ref, px_s.at[s], px_r.at[s], dev(x=1 - x)))
+        pool_to_x(ref, s)
+        pool_to_y(ref, s, x)
+    spread_x(UPS, late)
     mine = pl.ds(pl.multiple_of(me_fs * cols, cols), cols)
     for stream in (UPS, DOWNS):
         for p in range(most):
@@ -653,10 +666,18 @@
     upper_open = (lax.rem(offset + rows, SEQ_LEN) != 0).astype(f32)
     ext[0:HALO, :] = before[...].astype(f32) * lower_open
     ext[rows + HALO : rows + 2 * HALO, :] = after[...].astype(f32) * upper_open
-    for s in range(nz):
-        landed(pool_block(s, 1 - x), px_r.at[s])
-    go(rc(pool_full.at[mine_groups], pool_full.at[mine_groups], swap_s, swap_r, dev(c=1 - c)))
-    landed(pool_full.at[pl.ds((1 - c) * gpc, gpc)], swap_r)
+    for k in range(nz):
+        s = z if k == 0 else pick(NEAR, k - 1)
+        ref = pool_block(me, s, 1 - x)
+        landed(ref, px_r.at[s])
+        pool_to_y(ref, s, 1 - x)
+    pool_to_c(me, 0)
+    peer_c, peer_y, peer_yc = y * 2 + 1 - c, (1 - y) * 2 + c, (1 - y) * 2 + 1 - c
+    for f in range(2 * nz):
+        landed(pool_block(peer_y, f // 2, f % 2), py_r.at[f])
+    pool_to_c(peer_y, 1)
+    landed(pool_full.at[peer_c], pc_r.at[0])
+    landed(pool_full.at[peer_yc], pc_r.at[1])
 
     def rows_of(s, t):
         return pl.ds(pl.multiple_of(s * seq + t * rows, rows), rows)
@@ -680,60 +701,105 @@
         mixed = jnp.dot(pooled, pool_full[index], preferred_element_type=f32)
         first_all[my_rows, g] = (tok_ref[:, g].astype(f32) + mixed * scale_ref[:, g]).astype(bf)
 
-    def share(s, t, k, to):
-        ref = first_all.at[rows_of(s, t), :]
-        go(rc(ref, ref, f_s.at[k], f_r.at[k], to))
-
-    def shared(s, t, k):
-        landed(first_all.at[rows_of(s, t), :], f_r.at[k])
-
-    peer_y, peer_c = (1 - y) * 2 + c, y * 2 + 1 - c
-    peer_yc = (1 - y) * 2 + 1 - c
-    share(q, me, 0, dev(z=zp))
-    share(q, me, 1, dev(y=1 - y))
-    share(q, me, 3, dev(c=1 - c))
-    spread_z(DOWNS)
-    spread_x(DOWNS)
-    for k in range(3):
-        relay(UPS, k)
-
-    def norm_up(s, yy):
-        begin = s * seq + yy * 2 * rows
-
+    part_rows = rows // HALVES
+
+    def first_part(s, t, h):
+        return first_all.at[pl.ds(pl.multiple_of(s * seq + t * rows + h * part_rows, part_rows), part_rows), :]
+
+    def share(s, t, k, to, h):
+        ref = first_part(s, t, h)
+        go(rc(ref, ref, f_s.at[k * HALVES + h], f_r.at[k * HALVES + h], to))
+
+    def shared(s, t, k, h):
+        landed(first_part(s, t, h), f_r.at[k * HALVES + h])
+
+    halves = range(HALVES)
+    for h in halves:
+        share(q, me, 0, dev(z=zp), h)
+        share(q, me, 1, dev(y=1 - y), h)
+        share(q, me, 3, dev(c=1 - c), h)
+
+    def groups(s, yy):
+        return s * seq + yy * 2 * rows
+
+    def norm(begin):
         @pl.loop(0, 2 * rows // step)
         def _(i):
             r = pl.ds(pl.multiple_of(begin + i * step, step), step)
             v = first_all[r, :].astype(f32)
             v = v * lax.rsqrt(jnp.mean(v * v, axis=-1, keepdims=True) + EPS) * gmlp_ref[...]
-            inner[pl.ds(pl.multiple_of(i * step, step), step), :] = v.astype(bf)
-
-        @pl.loop(0, count_of(z))
+            inner_all[r, :] = v.astype(bf)
+
+    def up(begin, lo, hi):
+        g = pl.ds(pl.multiple_of(begin, 2 * rows), 2 * rows)
+
+        @pl.loop(lo, hi)
         def _(j):
             h = pl.ds(pl.multiple_of(j * piece, piece), piece)
             pre = lax.dot_general(
-                inner[...], up_full[h, :], (((1,), (1,)), ((), ())), preferred_element_type=f32
+                inner_all[g, :], up_full[h, :], (((1,), (1,)), ((), ())), preferred_element_type=f32
             )
-            hidden[pl.ds(pl.multiple_of(begin, 2 * rows), 2 * rows), h] = jnp.square(jnp.maximum(pre, 0.0)).astype(bf)
-
-    shared(1 - q, me, 0)
-    share(1 - q, me, 2, dev(y=1 - y))
-    share(1 - q, me, 4, dev(c=1 - c))
-    for s in range(nz):
-        from_x(UPS, s)
-    shared(q, peer_c, 3)
-    norm_up(q, y)
-    shared(q, peer_y, 1)
-    share(q, peer_y, 5, dev(c=1 - c))
-    shared(1 - q, peer_c, 4)
-    norm_up(1 - q, y)
-    relay(DOWNS, 0)
-    shared(q, peer_yc, 5)
-    norm_up(q, 1 - y)
-    relay(DOWNS, 1)
-    shared(1 - q, peer_y, 2)
-    share(1 - q, peer_y, 6, dev(c=1 - c))
-    shared(1 - q, peer_yc, 6)
-    norm_up(1 - q, 1 - y)
+            hidden[g, h] = jnp.square(jnp.maximum(pre, 0.0)).astype(bf)
+
+    def pull(pieces):
+        for p in pieces:
+            for k in range(3):
+                relay(UPS, k, (p,))
+
+    def ready(pieces):
+        for s in range(nz):
+            from_x(UPS, s, pieces)
+
+    def forward_z():
+        for h in halves:
+            shared(1 - q, me, 0, h)
+            share(1 - q, me, 2, dev(y=1 - y), h)
+            share(1 - q, me, 4, dev(c=1 - c), h)
+
+    def forward_y(s, k, kc):
+        for h in halves:
+            shared(s, peer_y, k, h)
+            share(s, peer_y, kc, dev(c=1 - c), h)
+
+    def from_c(s, t, k):
+        for h in halves:
+            shared(s, t, k, h)
+
+    g0, g1, g2, g3 = groups(q, y), groups(q, 1 - y), groups(1 - q, y), groups(1 - q, 1 - y)
+    quarter = most // 4
+    p0, p1, p2, p3 = [range(k * quarter, most if k == 3 else (k + 1) * quarter) for k in range(4)]
+    half = 2 * quarter
+    pull(p0)
+    from_c(q, peer_c, 3)
+    norm(g0)
+    pull(p1)
+    ready(p0)
+    ready(p1)
+    up(g0, 0, half)
+    spread_x(DOWNS, every)
+    forward_y(q, 1, 5)
+    from_c(q, peer_yc, 5)
+    norm(g1)
+    up(g1, 0, half)
+    pull(p2)
+    forward_z()
+    spread_z(DOWNS, [(p, k) for k in range(3) for p in every])
+    pull(p3)
+    from_c(1 - q, peer_c, 4)
+    norm(g2)
+    up(g2, 0, half)
+    ready(p2)
+    ready(p3)
+    up(g0, half, count_of(z))
+    up(g1, half, count_of(z))
+    up(g2, half, count_of(z))
+    relay(DOWNS, 0, every)
+    forward_y(1 - q, 2, 6)
+    from_c(1 - q, peer_yc, 6)
+    norm(g3)
+    up(g3, 0, count_of(z))
+    first_sends = list(pending)
+    pending.clear()
 
     chunk = 2 * rows
     orow = pl.ds(pl.multiple_of(q * seq, seq), seq)
@@ -750,33 +816,49 @@
         def _(i):
             body(pl.ds(pl.multiple_of(begin + i * fine, fine), fine), pl.ds(pl.multiple_of(i * fine, fine), fine))
 
+    def send_part(i, j):
+        plane, column, s, u = unit(i, j)
+        go(rc(part_send.at[s], part_recv.at[s], d_s.at[u], d_r.at[u], dev(c=1 - c)), lax.rem(plane, 2) != c)
+
+    def multiply(theirs, deep, cc, slots):
+        def all_rows(theirs, deep):
+            @pl.loop(0, 2 * seq // chunk)
+            def _(k):
+                r = pl.ds(pl.multiple_of(k * chunk, chunk), chunk)
+                value = jnp.dot(hidden[r, 0:deep], down_full[0:deep, cc], preferred_element_type=f32)
+                for n, s in enumerate(slots):
+                    lane = slice(n * cols, (n + 1) * cols)
+                    if theirs:
+                        part_send[s, r, :] = value[:, lane].astype(bf)
+                    else:
+                        part[s, r, :] = value[:, lane]
+
+        pl.when(theirs)(lambda: all_rows(True, deep))
+        pl.when(jnp.logical_not(theirs))(lambda: all_rows(False, deep))
+
+    def by_depth(body):
+        if ENDS == INNER:
+            body(ENDS * piece)
+        else:
+            pl.when(is_end(z))(lambda: body(ENDS * piece))
+            pl.when(jnp.logical_not(is_end(z)))(lambda: body(INNER * piece))
+
     def product(i, j):
         plane, column, s, u = unit(i, j)
         cc = pl.ds(pl.multiple_of((plane * 2 + column) * cols, cols), cols)
-        theirs = lax.rem(plane, 2) != c
         if j == 1:
-            from_x(DOWNS, plane)
-
-        def all_rows(depth_of):
-            @pl.loop(0, 2 * seq // chunk)
-            def _(k):
-                r = pl.ds(pl.multiple_of(k * chunk, chunk), chunk)
-                value = jnp.dot(hidden[r, 0:depth_of], down_full[0:depth_of, cc], preferred_element_type=f32)
-
-                @pl.when(theirs)
-                def _():
-                    part_send[s, r, :] = value.astype(bf)
-
-                @pl.when(jnp.logical_not(theirs))
-                def _():
-                    part[s, r, :] = value
-
-        if ENDS == INNER:
-            all_rows(ENDS * piece)
-        else:
-            pl.when(is_end(z))(lambda: all_rows(ENDS * piece))
-            pl.when(jnp.logical_not(is_end(z)))(lambda: all_rows(INNER * piece))
-        go(rc(part_send.at[s], part_recv.at[s], d_s.at[u], d_r.at[u], dev(c=1 - c)), theirs)
+            from_x(DOWNS, plane, every)
+        by_depth(lambda deep: multiply(lax.rem(plane, 2) != c, deep, cc, (s,)))
+        send_part(i, j)
+
+    def wide_product(i):
+        plane = jnp.where(z < 2, i, nz - 1 - i)
+        cc = pl.ds(pl.multiple_of(plane * 2 * cols, 2 * cols), 2 * cols)
+        from_x(DOWNS, plane, every)
+        slots = ((i // 2) * 2 + x, (i // 2) * 2 + 1 - x)
+        by_depth(lambda deep: multiply(lax.rem(plane, 2) != c, deep, cc, slots))
+        for j in (0, 1):
+            send_part(i, j)
 
     def stage1(i, j):
         plane, column, s, u = unit(i, j)
@@ -876,17 +958,29 @@
         for j in both:
             body(i, j)
 
-    for i in range(3):
-        run(product, i)
-        run(stage1, i)
-    for i in range(3):
-        run(stage2, i)
-    relay(DOWNS, 2)
+    def drain():
+        for copy, condition in pending:
+            guarded(condition, copy.wait_send)
+        pending.clear()
+
+    wide_product(0)
+    relay(DOWNS, 1, every)
+    wide_product(1)
+    run(stage1, 0)
+    run(stage1, 1)
+    wide_product(2)
+    run(stage1, 2)
+    relay(DOWNS, 2, every)
     run(product, 3)
+    run(stage2, 1)
     run(stage1, 3)
+    for copy, condition in first_sends:
+        guarded(condition, copy.wait_send)
+    run(stage2, 0)
+    run(stage2, 2)
+    run(stage2, 3)
     run(stage3, 0)
     run(stage3, 1)
-    run(stage2, 3)
     run(stage3, 2)
     run(stage3, 3)
 
@@ -895,8 +989,7 @@
     for d in range(1, tp):
         to = {"fs": me_fs, "tp": lax.rem(me + d, tp)}
         go(rc(stat_out, stat_in.at[d], st_s.at[d], st_r.at[d], to))
-    for copy, condition in pending:
-        guarded(condition, copy.wait_send)
+    drain()
     squares = stat_out[...]
     for d in range(1, tp):
         landed(stat_in.at[d], st_r.at[d])
@@ -932,7 +1025,7 @@
             pltpu.VMEM((deep, width), bf),
             pltpu.VMEM((rows + 2 * HALO, width), f32),
             pltpu.VMEM((2 * seq, width), bf),
-            pltpu.VMEM((2 * rows, width), bf),
+            pltpu.VMEM((2 * seq, width), bf),
             pltpu.VMEM((2 * seq, deep), bf),
             pltpu.VMEM((4, 2 * seq, cols), bf),
             pltpu.VMEM((4, 2 * seq, cols), bf),
@@ -946,10 +1039,10 @@
             pltpu.VMEM((seq, 128), f32),
             pltpu.VMEM((8, seq), f32),
             pltpu.VMEM((tp, 8, seq), f32),
-            dma((4,)), dma((4,)), dma((4,)), dma((4,)), dma, dma,
+            dma((4,)), dma((4,)), dma((4,)), dma((4,)), dma((8,)), dma((8,)), dma((2,)), dma((2,)),
             dma((lots,)), dma((lots,)), dma((lots,)), dma((lots,)),
             dma((2,)), dma((2,)),
-            dma((7,)), dma((7,)),
+            dma((7 * HALVES,)), dma((7 * HALVES,)),
             dma((8,)), dma((8,)), dma((8,)), dma((8,)), dma((8,)), dma((8,)),
             dma((tp,)), dma((tp,)),
         ],

time: 194 us -> 175 us (0.902)
  Pallas kernels: 192 us -> 173 us
    pallas_call x1, Pallas kernels: 192 us -> 173 us  [plane_local(): pl.pallas_call(plane_kernel, out_shape=jax.ShapeDtypeStruct((seq, own), b...]
where the time goes in v2:
time: 175 us
  Pallas kernels  173 us (99%)
  local copies, waits for them, and re-layouts  2.26 us (1%)
    pallas_call x1, Pallas kernels, plane_local(): pl.pallas_call(plane_kernel, out_shape=jax.ShapeDtypeStruct((seq, own), b...  173 us

profile of v2, /device:TPU:0, one launch (start us, length us, event | category | flops | bytes accessed | tf_op | source)
XLA Modules:
  0.0 175.2 jit_solution(10186457446228944635)
XLA Ops:
  0.0 172.9 %shard_map.82 = bf16[1024,512]{1,0:T(8,128)(2,1)} custom-call(bf16[256,2048]{1,0:T(8,128)(2,1)} %tok_ref.1, bf16[4,64,512]{2,1,0:T(8,128)(2,1)} %pool_ref.1, bf16[2048,256]{1,0:T(8,128)(2,1)} %up_ref.1, bf16[2048,256]{1,0:T(8,128)(2,1)} %down_ref.1, f32[1,2048]{1,0:T(1,128)} %bitcast.4, f32[1,2048]{1,0:T(1,128)} %bitcast.5, f32[1,2048]{1,0:T(1,128)} %bitcast.6, ...), custom_call_target="tpu_custom_call" | custom-call | tf_op jit(solution)/shard_map/pallas_call | solution.py:1017
  173.0 2.3 %copy.10 = bf16[1024,512]{1,0:T(8,128)(2,1)} copy(bf16[1024,512]{1,0:T(8,128)(2,1)} %shard_map.82) | data formatting | bytes 2097152

commit v3 on v2

--- a/solution.py
+++ b/solution.py
@@ -475,7 +475,8 @@
 
 NEAR = ((1, 2, 3), (0, 2, 3), (3, 1, 0), (2, 1, 0))
 TARGETS = ((1, 2, 3), (0, 3, 2), (3, 0, 1), (2, 1, 0))
-Y_FIRST = (True, False, True, False)
+DTARGETS = ((1, 2, 3), (0, 2, 3), (3, 1, 0), (2, 1, 0))
+Y_FIRST = ((True, True), (False, False), (True, False), (True, False))
 ENDS, INNER = 4, 4
 UPS, DOWNS = 0, 1
 HALVES = 2
@@ -588,7 +589,7 @@
 
     def spread_z(stream, order):
         for p, k in order:
-            t = pick(TARGETS, k)
+            t = pick(DTARGETS if stream else TARGETS, k)
             go(
                 rc(own_piece(stream, t, p), block(stream, z, x, p), wz_s.at[slot(stream, t, p)],
                    wz_r.at[slot(stream, z, p)], dev(z=t)),
@@ -782,18 +783,18 @@
     norm(g1)
     up(g1, 0, half)
     pull(p2)
+    spread_z(DOWNS, [(p, k) for k in range(3) for p in every])
     forward_z()
-    spread_z(DOWNS, [(p, k) for k in range(3) for p in every])
     pull(p3)
     from_c(1 - q, peer_c, 4)
     norm(g2)
     up(g2, 0, half)
     ready(p2)
+    relay(DOWNS, 0, every)
     ready(p3)
     up(g0, half, count_of(z))
     up(g1, half, count_of(z))
     up(g2, half, count_of(z))
-    relay(DOWNS, 0, every)
     forward_y(1 - q, 2, 6)
     from_c(1 - q, peer_yc, 6)
     norm(g3)
@@ -877,10 +878,10 @@
         @pl.when(ours)
         def _():
             landed(part_recv.at[s], d_r.at[u])
-            if not Y_FIRST[i]:
+            if not Y_FIRST[i][j]:
                 fold((1 - q) * seq, seq, False)
 
-        if Y_FIRST[i]:
+        if Y_FIRST[i][j]:
             pl.when(ours & home)(lambda: fold(0, 2 * seq, True))
             pl.when(ours & jnp.logical_not(home))(lambda: fold(0, 2 * seq, False))
             go(rc(part_recv.at[s], y_recv.at[j], y_s.at[u], y_r.at[u], dev(y=1 - y)), ours & jnp.logical_not(home))
@@ -892,7 +893,7 @@
         plane, column, s, u = unit(i, j)
         ours = lax.rem(plane, 2) == c
         home = lax.div(plane, 2) == y
-        if Y_FIRST[i]:
+        if Y_FIRST[i][j]:
             @pl.when(ours & home)
             def _():
                 landed(y_recv.at[j], y_r.at[u])
@@ -933,7 +934,7 @@
 
         @pl.when(plane == me)
         def _():
-            if Y_FIRST[i]:
+            if Y_FIRST[i][j]:
                 landed(z_recv.at[s], z_r.at[u])
             else:
                 landed(y_recv.at[j, orow, :], y_r.at[u])
@@ -941,7 +942,7 @@
             cc = pl.ds(pl.multiple_of(me * own_cols + column * cols, cols), cols)
 
             def body(r, l):
-                more = z_recv[s, l, :] if Y_FIRST[i] else y_recv[j, r, :]
+                more = z_recv[s, l, :] if Y_FIRST[i][j] else y_recv[j, r, :]
                 value = part[s, r, :] + more.astype(f32) + first_all[r, cc].astype(f32)
                 total[l, here] = value
                 square = value * value

time: 175 us -> 168 us (0.960)
  Pallas kernels: 173 us -> 165 us
    pallas_call x1, Pallas kernels: 173 us -> 165 us  [plane_local(): pl.pallas_call(plane_kernel, out_shape=jax.ShapeDtypeStruct((seq, own), b...]
where the time goes in v3:
time: 168 us; the launch traced here: 167 us
  Pallas kernels  165 us (98%)
  local copies, waits for them, and re-layouts  2.26 us (1%)
    pallas_call x1, Pallas kernels, plane_local(): pl.pallas_call(plane_kernel, out_shape=jax.ShapeDtypeStruct((seq, own), b...  165 us

profile of v3, /device:TPU:0, one launch (start us, length us, event | category | flops | bytes accessed | tf_op | source)
XLA Modules:
  0.0 167.4 jit_solution(14340542867418726844)
XLA Ops:
  0.0 165.1 %shard_map.82 = bf16[1024,512]{1,0:T(8,128)(2,1)} custom-call(bf16[256,2048]{1,0:T(8,128)(2,1)} %tok_ref.1, bf16[4,64,512]{2,1,0:T(8,128)(2,1)} %pool_ref.1, bf16[2048,256]{1,0:T(8,128)(2,1)} %up_ref.1, bf16[2048,256]{1,0:T(8,128)(2,1)} %down_ref.1, f32[1,2048]{1,0:T(1,128)} %bitcast.4, f32[1,2048]{1,0:T(1,128)} %bitcast.5, f32[1,2048]{1,0:T(1,128)} %bitcast.6, ...), custom_call_target="tpu_custom_call" | custom-call | tf_op jit(solution)/shard_map/pallas_call | solution.py:1018
  165.1 2.3 %copy.10 = bf16[1024,512]{1,0:T(8,128)(2,1)} copy(bf16[1024,512]{1,0:T(8,128)(2,1)} %shard_map.82) | data formatting | bytes 2097152

commit v4 on v3

--- a/solution.py
+++ b/solution.py
@@ -784,8 +784,8 @@
     up(g1, 0, half)
     pull(p2)
     spread_z(DOWNS, [(p, k) for k in range(3) for p in every])
+    pull(p3)
     forward_z()
-    pull(p3)
     from_c(1 - q, peer_c, 4)
     norm(g2)
     up(g2, 0, half)

time: 168 us -> 168 us (level)
  no operation moved by 1% of the time
where the time goes in v4:
time: 168 us; the launch traced here: 167 us
  Pallas kernels  165 us (98%)
  local copies, waits for them, and re-layouts  2.26 us (1%)
    pallas_call x1, Pallas kernels, plane_local(): pl.pallas_call(plane_kernel, out_shape=jax.ShapeDtypeStruct((seq, own), b...  165 us

profile of v4, /device:TPU:0, one launch (start us, length us, event | category | flops | bytes accessed | tf_op | source)
XLA Modules:
  0.0 167.4 jit_solution(5424843617402348950)
XLA Ops:
  0.0 165.1 %shard_map.82 = bf16[1024,512]{1,0:T(8,128)(2,1)} custom-call(bf16[256,2048]{1,0:T(8,128)(2,1)} %tok_ref.1, bf16[4,64,512]{2,1,0:T(8,128)(2,1)} %pool_ref.1, bf16[2048,256]{1,0:T(8,128)(2,1)} %up_ref.1, bf16[2048,256]{1,0:T(8,128)(2,1)} %down_ref.1, f32[1,2048]{1,0:T(1,128)} %bitcast.4, f32[1,2048]{1,0:T(1,128)} %bitcast.5, f32[1,2048]{1,0:T(1,128)} %bitcast.6, ...), custom_call_target="tpu_custom_call" | custom-call | tf_op jit(solution)/shard_map/pallas_call | solution.py:1018
  165.1 2.3 %copy.10 = bf16[1024,512]{1,0:T(8,128)(2,1)} copy(bf16[1024,512]{1,0:T(8,128)(2,1)} %shard_map.82) | data formatting | bytes 2097152
